TPU v7x, 32 devices: a whole 2x2x4 slice. The times are simulated.
32 devices in a mesh: ep: 4 (over y, x), tp: 8 (over z, core).
Axes of the slice: x: 2, y: 2, z: 4, core: 2. Of those that a mesh axis runs over, the one named last changes fastest.
Arguments:
- queries: bfloat16 [4096, 1024], P('ep', 'tp'), may hold values from -600 to 600
- key_rows: bfloat16 [4096, 128], P('ep'), may hold values from -6 to 6
- value_rows: bfloat16 [4096, 128], P('ep'), may hold values from -48 to 48
- sink_logits: float32 [16], P('tp'), may hold values from 2 to 6
- out_weight: bfloat16 [1024, 2048], P('tp'), may hold values from -0.1875 to 0.1875
- moe_rows: bfloat16 [1024, 2048], P(('ep', 'tp')), may hold values from -6 to 6
- moe_gain: float32 [2048], replicated, may hold values from 0.1 to 1.9
- routes: int32 [1024, 2], P(('ep', 'tp')), may hold values from 0 to 3, all different within a row; in each aligned block of 32 rows (0 to 31, 32 to 63, ...) at most 24 rows name the same one
- route_weight: float32 [1024, 2], P(('ep', 'tp')), may hold values from 0.2 to 1
- gate_weight: bfloat16 [4, 2048, 7168], P('ep', None, 'tp'), may hold values from -0.125 to 0.125
- up_weight: bfloat16 [4, 2048, 7168], P('ep', None, 'tp'), may hold values from -0.125 to 0.125
- down_weight: bfloat16 [4, 7168, 2048], P('ep', 'tp'), may hold values from -0.0625 to 0.0625
Outputs:
- mixer_out: bfloat16 [4096, 2048], P(('ep', 'tp'))
- moe_out: bfloat16 [1024, 2048], P(('ep', 'tp'))
Inputs may be any that keep to these rules, and one draw needn't show every extreme that they name: `routes`: in each aligned block of 32 rows (the rows of one device) no expert is named more than 24 times, a bound that some block reaches; each row names 2 different experts.
All inputs are finite; a program needn't handle non-finite values.
Results may differ from a plain program's by a relative error of at most 0.02.
Values may be sent and summed in bfloat16 or wider, within the bound.
A program may use at most 128 MiB of HBM per device.

v0:
```python
import jax
import jax.numpy as jnp
from jax import lax
from jax.sharding import PartitionSpec as P

HEADS = 16
KV_HEADS = 2
HEAD_DIM = 64
WINDOW = 128
TOP = 2
big_negative = -1e30
norm_eps = 1e-05


def passed_along(value, axis, steps):
    count = lax.axis_size(axis)
    initial, last = (max(0, -steps), min(count, count - steps))
    return lax.ppermute(value, axis, [(source, source + steps) for source in range(initial, last)])


def layer_normed(inputs, gain):
    values = inputs.astype(jnp.float32)
    center = values - jnp.mean(values, -1, keepdims=True)
    spread = jnp.mean(center * center, -1, keepdims=True)
    return (center * lax.rsqrt(spread + norm_eps) * gain).astype(jnp.bfloat16)


def attend(queries, key_rows, value_rows, sink_logits):
    total = queries.shape[0]
    heads_here = sink_logits.shape[0]
    blocks = total // WINDOW
    key_head = lax.axis_index("tp") * heads_here // (HEADS // KV_HEADS)
    key_own = lax.dynamic_slice_in_dim(key_rows, key_head * HEAD_DIM, HEAD_DIM, 1)
    value_own = lax.dynamic_slice_in_dim(value_rows, key_head * HEAD_DIM, HEAD_DIM, 1)
    last_rows = jnp.concatenate([key_own[total - WINDOW :], value_own[total - WINDOW :]], 1)
    earlier = passed_along(last_rows, "ep", 1)
    key_ext = jnp.concatenate([earlier[:, :HEAD_DIM], key_own], 0)
    value_ext = jnp.concatenate([earlier[:, HEAD_DIM:], value_own], 0)
    key_blocks = jnp.concatenate(
        [
            key_ext[:total].reshape(blocks, WINDOW, HEAD_DIM),
            key_ext[WINDOW:].reshape(blocks, WINDOW, HEAD_DIM),
        ],
        1,
    )
    value_blocks = jnp.concatenate(
        [
            value_ext[:total].reshape(blocks, WINDOW, HEAD_DIM),
            value_ext[WINDOW:].reshape(blocks, WINDOW, HEAD_DIM),
        ],
        1,
    )
    query_blocks = queries.reshape(blocks, WINDOW, heads_here, HEAD_DIM)
    scores = jnp.einsum(
        "nqhd,nkd->nhqk", query_blocks, key_blocks, preferred_element_type=jnp.float32
    ) * HEAD_DIM ** (-0.5)
    anchor = lax.axis_index("ep") * total
    block_base = anchor + jnp.arange(blocks, dtype=jnp.int32)[:, None, None] * WINDOW
    query_pos = block_base + jnp.arange(WINDOW, dtype=jnp.int32)[None, :, None]
    key_pos = block_base - WINDOW + jnp.arange(2 * WINDOW, dtype=jnp.int32)[None, None, :]
    allowed = ((key_pos <= query_pos) & (key_pos > query_pos - WINDOW) & (key_pos >= 0))[:, None]
    masked = jnp.where(allowed, scores, big_negative)
    sinks = sink_logits[None, :, None]
    row_max = jnp.maximum(jnp.max(masked, -1), sinks)
    powers = jnp.where(allowed, jnp.exp(masked - row_max[..., None]), 0.0)
    totals = jnp.sum(powers, -1) + jnp.exp(sinks - row_max)
    attn_probs = (powers / totals[..., None]).astype(jnp.bfloat16)
    attended = jnp.einsum(
        "nhqk,nkd->nqhd", attn_probs, value_blocks, preferred_element_type=jnp.float32
    )
    return attended.astype(jnp.bfloat16).reshape(total, heads_here * HEAD_DIM)


def mixer(queries, key_rows, value_rows, sink_logits, out_weight):
    attended = attend(queries, key_rows, value_rows, sink_logits)
    return lax.psum_scatter(
        jnp.dot(attended, out_weight, preferred_element_type=jnp.float32).astype(jnp.bfloat16),
        "tp",
        scatter_dimension=0,
        tiled=True,
    )


def experts(moe_rows, moe_gain, routes, route_weight, gate_weight, up_weight, down_weight):
    row_count = moe_rows.shape[0]
    width_all = moe_rows.shape[1]
    expert_count = gate_weight.shape[0] * lax.axis_size("ep")
    capacity = 3 * row_count * TOP // (2 * expert_count)
    normed = layer_normed(moe_rows, moe_gain)
    chosen = routes.reshape(-1)
    onehot = (chosen[:, None] == jnp.arange(expert_count, dtype=jnp.int32)[None, :]).astype(
        jnp.int32
    )
    earlier_count = jnp.cumsum(onehot, 0) - onehot
    slot_index = jnp.sum(earlier_count * onehot, 1)
    target = chosen * capacity + slot_index
    matches = target[None, :] == jnp.arange(expert_count * capacity, dtype=jnp.int32)[:, None]
    dispatch_map = jnp.sum(matches.reshape(expert_count * capacity, row_count, TOP), -1).astype(
        jnp.bfloat16
    )
    buffer = jnp.dot(dispatch_map, normed, preferred_element_type=jnp.float32).astype(jnp.bfloat16)
    buffer = buffer.reshape(expert_count, capacity, width_all)
    gate_mat = gate_weight[0]
    up_mat = up_weight[0]
    down_mat = down_weight[0]
    received = lax.all_to_all(buffer, "ep", split_axis=0, concat_axis=0, tiled=True)
    total = received.shape[0] * received.shape[1]
    flat_rows = received.reshape(total, width_all)
    shard_rows = lax.all_gather(flat_rows, "tp", axis=0, tiled=True)
    gate_val = jnp.dot(shard_rows, gate_mat, preferred_element_type=jnp.float32)
    up_val = jnp.dot(shard_rows, up_mat, preferred_element_type=jnp.float32)
    hidden = (jax.nn.silu(gate_val) * up_val).astype(jnp.bfloat16)
    summed = lax.psum_scatter(
        jnp.dot(hidden, down_mat, preferred_element_type=jnp.float32).astype(jnp.bfloat16),
        "tp",
        scatter_dimension=0,
        tiled=True,
    )
    results = summed.reshape(received.shape)
    returned = lax.all_to_all(results, "ep", split_axis=0, concat_axis=0, tiled=True)
    weights_flat = route_weight.reshape(-1)
    combine_map = jnp.sum(
        jnp.where(matches, weights_flat[None, :], 0.0).reshape(
            expert_count * capacity, row_count, TOP
        ),
        -1,
    )
    returned_flat = returned.reshape(expert_count * capacity, width_all).astype(jnp.float32)
    moe_out = lax.dot_general(
        combine_map, returned_flat, (((0,), (0,)), ((), ())), precision=lax.Precision.HIGHEST
    )
    return moe_out.astype(jnp.bfloat16)


def dense_experts(moe_rows, moe_gain, routes, route_weight, gate_weight, up_weight, down_weight):
    count = lax.axis_size("ep")
    normed = layer_normed(moe_rows, moe_gain)
    both = ("ep", "tp")
    rows = lax.all_gather(normed, both, axis=0, tiled=True)
    named = routes[:, :, None] == jnp.arange(count, dtype=jnp.int32)[None, None, :]
    shares = jnp.sum(jnp.where(named, route_weight[:, :, None], 0.0), 1)
    shares = lax.all_gather(shares, both, axis=0, tiled=True)
    share = lax.dynamic_slice_in_dim(shares, lax.axis_index("ep"), 1, 1)
    gate_val = jnp.dot(rows, gate_weight[0], preferred_element_type=jnp.float32)
    up_val = jnp.dot(rows, up_weight[0], preferred_element_type=jnp.float32)
    hidden = (jax.nn.silu(gate_val) * up_val).astype(jnp.bfloat16)
    down = jnp.dot(hidden, down_weight[0], preferred_element_type=jnp.float32)
    return lax.psum_scatter(
        (down * share).astype(jnp.bfloat16), both, scatter_dimension=0, tiled=True
    )


def body(
    queries,
    key_rows,
    value_rows,
    sink_logits,
    out_weight,
    moe_rows,
    moe_gain,
    routes,
    route_weight,
    gate_weight,
    up_weight,
    down_weight,
):
    mixer_out = mixer(queries, key_rows, value_rows, sink_logits, out_weight)
    slots = 3 * moe_rows.shape[0] * TOP // 2
    sparse = (
        slots * lax.axis_size("tp")
        < moe_rows.shape[0] * lax.axis_size("tp") * lax.axis_size("ep") // 2
    )
    layer = experts if sparse else dense_experts
    moe_out = layer(moe_rows, moe_gain, routes, route_weight, gate_weight, up_weight, down_weight)
    return (mixer_out, moe_out)


def solution(mesh):
    in_specs = (
        P("ep", "tp"),
        P("ep", None),
        P("ep", None),
        P("tp"),
        P("tp", None),
        P(("ep", "tp"), None),
        P(),
        P(("ep", "tp"), None),
        P(("ep", "tp"), None),
        P("ep", None, "tp"),
        P("ep", None, "tp"),
        P("ep", "tp", None),
    )
    out_specs = (P(("ep", "tp"), None), P(("ep", "tp"), None))
    return jax.shard_map(body, mesh=mesh, in_specs=in_specs, out_specs=out_specs, check_vma=False)
```

profile of v0, /device:TPU:0, one launch (start us, length us, event | category | flops | bytes accessed | tf_op | source)
XLA Modules:
  0.0 265.6 jit_solution(14966716993027986457)
XLA Ops:
  8.1 1.1 convert_reduce_fusion
  9.1 1.1 fusion.14
  10.3 1.7 fusion.16
  12.0 0.8 dynamic-slice
  12.9 0.8 dynamic-slice.1
  13.7 0.1 pad_maximum_fusion.2
  13.8 4.9 %collective-permute-start = (bf16[128,128]{1,0:T(8,128)(2,1)S(1)}, bf16[128,128]{1,0:T(8,128)(2,1)S(1)}, u32[]{:S(2)}, u32[]{:S(2)}) collective-permute-start(bf16[128,128]{1,0:T(8,128)(2,1)S(1)} %pad_maximum_fusion.2), channel_id=1, source_target_pairs={{0,8},{8,16},{16,24},{1,9},{9,17},{17,25},{2,10},{10,18},{18,26},{... | collective-permute-start | bytes 98312 | tf_op jit(solution)/shard_map/ppermute | solution.py:18
  18.7 0.1 broadcast_compare_fusion
  18.9 0.1 iota_add_fusion.1
  19.0 0.7 and_and_fusion
  19.7 1.2 constant_dynamic-slice_fusion.1
  20.9 0.1 copy.55
  21.1 0.1 copy.51
  21.2 1.2 reshape.156
  22.4 0.1 fusion.28
  22.6 0.1 copy.50
  22.8 0.1 copy.54
  22.9 0.6 fusion.7
  23.5 0.1 broadcast_maximum_fusion
  23.6 0.6 fusion.8
  24.2 0.1 exponential_add_fusion
  24.3 0.7 fusion.9
  25.0 0.2 copy.59
  25.2 3.2 %convolution_convert_fusion = bf16[1024,2048]{1,0:T(8,128)(2,1)} fusion(bf16[128,2048]{1,0:T(8,128)(2,1)S(1)} %copy-done, bf16[16,8,8,128]{3,2,1,0:T(8,128)(2,1)S(1)} %bitcast.57), kind=kOutput, calls=%fused_computation.1 | convolution fusion | flops 538968064 | bytes 4980736 | tf_op jit(solution)/shard_map/dot_general | solution.py:77
  28.5 0.6 copy-done.2
  29.1 42.2 %all-gather = f32[32,32,4]{1,2,0:T(4,128)S(1)} all-gather(f32[1,32,4]{1,2,0:T(4,128)S(1)} %bitcast.60), channel_id=1, replica_groups=mesh['ep'=4,'tp'=8] {'ep','tp'}, dimensions={0}, use_global_device_ids=true | all-gather | bytes 16896 | tf_op jit(solution)/shard_map/all_gather | solution.py:142
  71.3 0.1 reshape.153
  71.4 25.5 %all-gather.3.cloned.1.call-done = bf16[1024,2048]{1,0:T(8,128)(2,1)} async-done(((bf16[32,2048]{1,0:T(8,128)(2,1)}), bf16[1024,2048]{1,0:T(8,128)(2,1)}) %all-gather.3.cloned.1.call-update) | async-done | bytes 4194320 | tf_op jit(solution)/shard_map/all_gather | solution.py:139
  97.0 7.5 %fusion.1 = f32[1024,896]{1,0:T(8,128)S(1)} fusion(bf16[1024,2048]{1,0:T(8,128)(2,1)} %all-gather.3.cloned.1.call-done, bf16[1,2048,896]{2,1,0:T(8,128)(2,1)} %param.22), kind=kOutput, calls=%fused_computation.3 | convolution fusion | flops 3758096384 | bytes 11534336 | tf_op jit(solution)/shard_map/dot_general | solution.py:145
  104.5 4.8 %multiply_convert_fusion.1 = bf16[1024,896]{1,0:T(8,128)(2,1)S(1)} fusion(f32[1024,896]{1,0:T(8,128)S(1)} %fusion.1, bf16[1024,2048]{1,0:T(8,128)(2,1)S(1)} %copy-done.4, bf16[1,2048,896]{2,1,0:T(8,128)(2,1)S(1)} %copy-done.5), kind=kOutput, calls=%fused_computation.7 | convolution fusion | flops 3763601408 | bytes 13369344 | tf_op jit(solution)/shard_map/dot_general | solution.py:144
  109.3 6.1 %multiply_convert_fusion = bf16[1024,2048]{1,0:T(8,128)(2,1)} fusion(bf16[1024,896]{1,0:T(8,128)(2,1)S(1)} %multiply_convert_fusion.1, f32[1024]{0:T(1024)S(1)} %bitcast.61, bf16[1,896,2048]{2,1,0:T(8,128)(2,1)S(1)} %copy-done.6), kind=kOutput, calls=%fused_computation | convolution fusion | flops 3762290688 | bytes 9703424 | tf_op jit(solution)/shard_map/dot_general | solution.py:147
  115.4 142.8 %reduce-scatter.5.cloned.1.call-done = bf16[32,2048]{1,0:T(8,128)(2,1)} async-done(((bf16[1024,2048]{1,0:T(8,128)(2,1)}), bf16[32,2048]{1,0:T(8,128)(2,1)}) %reduce-scatter.5.cloned.1.call-update) | async-done | bytes 131088 | tf_op jit(solution)/shard_map/reduce_scatter | solution.py:148
  (30 shorter events, 0.5 us)
Async XLA Ops:
  8.0 17.2 %copy-start = (bf16[128,2048]{1,0:T(8,128)(2,1)S(1)}, bf16[128,2048]{1,0:T(8,128)(2,1)}, u32[]{:S(2)}) copy-start(bf16[128,2048]{1,0:T(8,128)(2,1)} %param.16) | copy-start | bytes 1572868
  8.0 89.0 %all-gather.3.cloned.1.call-start = ((), (), s32[]{:S(2)}) async-start(), calls=%async_computation.3 | async-start | bytes 4325376 | tf_op jit(solution)/shard_map/all_gather | solution.py:139
  12.0 103.4 %reduce-scatter.3.cloned.1.call-start = ((), (), s32[]{:S(2)}) async-start(), calls=%async_computation.2 | async-start | bytes 4718592 | tf_op jit(solution)/shard_map/reduce_scatter | solution.py:76
  13.8 8.6 %collective-permute-start = (bf16[128,128]{1,0:T(8,128)(2,1)S(1)}, bf16[128,128]{1,0:T(8,128)(2,1)S(1)}, u32[]{:S(2)}, u32[]{:S(2)}) collective-permute-start(bf16[128,128]{1,0:T(8,128)(2,1)S(1)} %pad_maximum_fusion.2), channel_id=1, source_target_pairs={{0,8},{8,16},{16,24},{1,9},{9,17},{17,25},{2,10},{10,18},{18,26},{... | collective-permute-start | bytes 98312 | tf_op jit(solution)/shard_map/ppermute | solution.py:18
  20.9 2.6 copy-start.1
  28.4 0.7 copy-start.2
  28.4 0.7 copy-start.3
  28.4 229.8 %reduce-scatter.5.cloned.1.call-start = ((), (), s32[]{:S(2)}) async-start(), calls=%async_computation.4 | async-start | bytes 4325376 | tf_op jit(solution)/shard_map/reduce_scatter | solution.py:148
  97.0 7.5 %copy-start.4 = (bf16[1024,2048]{1,0:T(8,128)(2,1)S(1)}, bf16[1024,2048]{1,0:T(8,128)(2,1)}, u32[]{:S(2)}) copy-start(bf16[1024,2048]{1,0:T(8,128)(2,1)} %all-gather.3.cloned.1.call-done) | copy-start | bytes 12582916
  97.0 7.5 %copy-start.5 = (bf16[1,2048,896]{2,1,0:T(8,128)(2,1)S(1)}, bf16[1,2048,896]{2,1,0:T(8,128)(2,1)}, u32[]{:S(2)}) copy-start(bf16[1,2048,896]{2,1,0:T(8,128)(2,1)} %param.21) | copy-start | bytes 11010052
  104.5 4.8 %copy-start.6 = (bf16[1,896,2048]{2,1,0:T(8,128)(2,1)S(1)}, bf16[1,896,2048]{2,1,0:T(8,128)(2,1)}, u32[]{:S(2)}) copy-start(bf16[1,896,2048]{2,1,0:T(8,128)(2,1)} %param.23) | copy-start | bytes 11010052
Sparse Core Ops, SparseCore 0:
  12.4 84.5 all-gather.2
Sparse Core Ops, SparseCore 1:
  28.5 64.4 reduce-scatter.2
  115.5 142.7 reduce-scatter.4
where the time goes:
time: 266 us
  waiting for transfers between devices  168 us (63%)
  blocking collectives  42.2 us (16%)
  matrix products  22.9 us (9%)
  between operations  15.7 us (6%)
  other arithmetic  5.77 us (2%)
  local copies, waits for them, and re-layouts  5.72 us (2%)
  starting transfers between devices  5 us (2%)
    reduce_scatter x1, waiting for transfers between devices, dense_experts(): lax.psum_scatter((down * share).astype(jnp.bfloat16), both, scatter_dimen...  143 us
    all_gather x1, blocking collectives, dense_experts(): shares = lax.all_gather(shares, both, axis=0, tiled=True)  42.2 us
    all_gather x1, waiting for transfers between devices, dense_experts(): rows = lax.all_gather(normed, both, axis=0, tiled=True)  25.5 us
    dot_general x1, matrix products, dense_experts(): up_val = jnp.dot(rows, up_weight[0], preferred_element_type=jnp.float32)  7.49 us
    dot_general x1, matrix products, dense_experts(): down = jnp.dot(hidden, down_weight[0], preferred_element_type=jnp.float32)  6.08 us
  transfers between devices with their start and end apart: 4, of which 2 were waited for; matrix products, arithmetic and copies ran while one was open for 11% of the time, Pallas kernels for 0%

commit v1 on v0

--- a/solution.py
+++ b/solution.py
@@ -136,10 +136,15 @@
     count = lax.axis_size("ep")
     normed = layer_normed(moe_rows, moe_gain)
     both = ("ep", "tp")
-    rows = lax.all_gather(normed, both, axis=0, tiled=True)
     named = routes[:, :, None] == jnp.arange(count, dtype=jnp.int32)[None, None, :]
     shares = jnp.sum(jnp.where(named, route_weight[:, :, None], 0.0), 1)
-    shares = lax.all_gather(shares, both, axis=0, tiled=True)
+    rows, shares = jnp.split(
+        jax.lax.all_gather(
+            jnp.concatenate([normed, shares], axis=1), axis_name=both, axis=0, tiled=True
+        ),
+        [normed.shape[1]],
+        axis=1,
+    )
     share = lax.dynamic_slice_in_dim(shares, lax.axis_index("ep"), 1, 1)
     gate_val = jnp.dot(rows, gate_weight[0], preferred_element_type=jnp.float32)
     up_val = jnp.dot(rows, up_weight[0], preferred_element_type=jnp.float32)

time: 266 us -> 288 us (1.083)
  waiting for transfers between devices: 168 us -> 231 us
  blocking collectives: 42.2 us -> 0 us
    all_gather x1, waiting for transfers between devices: 25.5 us -> 87.7 us  [dense_experts(): jax.lax.all_gather(jnp.concatenate([normed, shares], axis=1), axis_name=b...]
    all_gather x1 -> x0, blocking collectives: 42.2 us -> none  [dense_experts(): shares = lax.all_gather(shares, both, axis=0, tiled=True)]
where the time goes in v1:
time: 288 us; the launch traced here: 287 us
  waiting for transfers between devices  231 us (80%)
  matrix products  23.6 us (8%)
  between operations  15.8 us (5%)
  other arithmetic  6.59 us (2%)
  local copies, waits for them, and re-layouts  5.58 us (2%)
  starting transfers between devices  5 us (2%)
    reduce_scatter x1, waiting for transfers between devices, dense_experts(): lax.psum_scatter((down * share).astype(jnp.bfloat16), both, scatter_dimen...  143 us
    all_gather x1, waiting for transfers between devices, dense_experts(): jax.lax.all_gather(jnp.concatenate([normed, shares], axis=1), axis_name=b...  87.7 us
    dot_general x1, matrix products, dense_experts(): up_val = jnp.dot(rows, up_weight[0], preferred_element_type=jnp.float32)  8.19 us
    dot_general x1, matrix products, dense_experts(): down = jnp.dot(hidden, down_weight[0], preferred_element_type=jnp.float32)  6.04 us
  transfers between devices with their start and end apart: 4, of which 2 were waited for; matrix products, arithmetic and copies ran while one was open for 11% of the time, Pallas kernels for 0%

profile of v1, /device:TPU:0, one launch (start us, length us, event | category | flops | bytes accessed | tf_op | source)
XLA Modules:
  0.0 287.5 jit_solution(13802841040865803329)
XLA Ops:
  8.1 1.1 convert_reduce_fusion
  9.2 1.1 fusion.18
  10.3 0.7 select_reduce_fusion
  11.0 0.1 copy.44
  11.1 1.0 fusion.27
  12.1 0.8 pad_maximum_fusion
  13.0 0.8 dynamic-slice
  13.8 0.8 dynamic-slice.1
  14.7 0.1 pad_maximum_fusion.3
  14.8 4.9 %collective-permute-start = (bf16[128,128]{1,0:T(8,128)(2,1)S(1)}, bf16[128,128]{1,0:T(8,128)(2,1)S(1)}, u32[]{:S(2)}, u32[]{:S(2)}) collective-permute-start(bf16[128,128]{1,0:T(8,128)(2,1)S(1)} %pad_maximum_fusion.3), channel_id=1, source_target_pairs={{0,8},{8,16},{16,24},{1,9},{9,17},{17,25},{2,10},{10,18},{18,26},{... | collective-permute-start | bytes 98312 | tf_op jit(solution)/shard_map/ppermute | solution.py:18
  19.7 0.1 broadcast_compare_fusion
  19.9 0.7 and_and_fusion
  20.6 1.2 constant_dynamic-slice_fusion
  21.9 0.1 copy.39
  22.0 0.1 copy.35
  22.2 0.2 reshape.154
  22.4 0.1 fusion.33
  22.6 0.1 copy.34
  22.8 0.1 copy.38
  22.9 0.6 fusion.11
  23.6 0.6 fusion.12
  24.2 0.1 exponential_add_fusion
  24.2 0.7 fusion.13
  25.0 0.2 copy.43
  25.2 3.3 %convolution_convert_fusion = bf16[1024,2048]{1,0:T(8,128)(2,1)} fusion(bf16[128,2048]{1,0:T(8,128)(2,1)S(1)} %copy-done, bf16[16,8,8,128]{3,2,1,0:T(8,128)(2,1)S(1)} %bitcast.51), kind=kOutput, calls=%fused_computation.5 | convolution fusion | flops 538968064 | bytes 4980736 | tf_op jit(solution)/shard_map/dot_general | solution.py:77
  28.5 87.7 %all-gather.2.cloned.1.call-done = f32[1024,2052]{1,0:T(8,128)} async-done(((f32[32,2052]{1,0:T(8,128)}), f32[1024,2052]{1,0:T(8,128)}) %all-gather.2.cloned.1.call-update) | async-done | bytes 8405008 | tf_op jit(solution)/shard_map/all_gather | solution.py:142
  116.2 1.1 split.9
  117.3 0.4 dynamic-slice_reduce_fusion
  117.7 8.2 %fusion = f32[1024,896]{1,0:T(8,128)S(1)} fusion(f32[1024,2052]{1,0:T(8,128)} %all-gather.2.cloned.1.call-done, bf16[1,2048,896]{2,1,0:T(8,128)(2,1)} %param.22), kind=kOutput, calls=%fused_computation.1 | convolution fusion | flops 3758096384 | bytes 11534336 | tf_op jit(solution)/shard_map/dot_general | solution.py:150
  125.9 4.8 %multiply_convert_fusion.1 = bf16[1024,896]{1,0:T(8,128)(2,1)S(1)} fusion(f32[1024,896]{1,0:T(8,128)S(1)} %fusion, bf16[1,2048,896]{2,1,0:T(8,128)(2,1)S(1)} %copy-done.3, f32[1024,2052]{1,0:T(8,128)S(1)} %bitcast.55), kind=kOutput, calls=%fused_computation.9 | convolution fusion | flops 3763601408 | bytes 13369344 | tf_op jit(solution)/shard_map/dot_general | solution.py:149
  130.8 6.0 %multiply_convert_fusion = bf16[1024,2048]{1,0:T(8,128)(2,1)} fusion(bf16[1024,896]{1,0:T(8,128)(2,1)S(1)} %multiply_convert_fusion.1, f32[1024]{0:T(1024)S(1)} %dynamic-slice_reduce_fusion, bf16[1,896,2048]{2,1,0:T(8,128)(2,1)S(1)} %copy-done.4), kind=kOutput, calls=%fused_computation | convolution fusion | flops 3762290688 | bytes 9703424 | tf_op jit(solution)/shard_map/dot_general | solution.py:152
  136.9 143.2 %reduce-scatter.5.cloned.1.call-done = bf16[32,2048]{1,0:T(8,128)(2,1)} async-done(((bf16[1024,2048]{1,0:T(8,128)(2,1)}), bf16[32,2048]{1,0:T(8,128)(2,1)}) %reduce-scatter.5.cloned.1.call-update) | async-done | bytes 131088 | tf_op jit(solution)/shard_map/reduce_scatter | solution.py:153
  (33 shorter events, 0.6 us)
Async XLA Ops:
  8.0 17.2 %copy-start = (bf16[128,2048]{1,0:T(8,128)(2,1)S(1)}, bf16[128,2048]{1,0:T(8,128)(2,1)}, u32[]{:S(2)}) copy-start(bf16[128,2048]{1,0:T(8,128)(2,1)} %param.16) | copy-start | bytes 1572868
  8.0 14.2 %copy-start.1 = (bf16[1024,128]{1,0:T(8,128)(2,1)S(1)}, bf16[1024,128]{1,0:T(8,128)(2,1)}, u32[]{:S(2)}) copy-start(bf16[1024,128]{1,0:T(8,128)(2,1)} %param.12) | copy-start | bytes 786436
  8.0 108.2 %all-gather.2.cloned.1.call-start = ((), (), s32[]{:S(2)}) async-start(), calls=%async_computation.3 | async-start | bytes 9191424 | tf_op jit(solution)/shard_map/all_gather | solution.py:142
  12.9 123.9 %reduce-scatter.3.cloned.1.call-start = ((), (), s32[]{:S(2)}) async-start(), calls=%async_computation.2 | async-start | bytes 4718592 | tf_op jit(solution)/shard_map/reduce_scatter | solution.py:76
  14.8 7.7 %collective-permute-start = (bf16[128,128]{1,0:T(8,128)(2,1)S(1)}, bf16[128,128]{1,0:T(8,128)(2,1)S(1)}, u32[]{:S(2)}, u32[]{:S(2)}) collective-permute-start(bf16[128,128]{1,0:T(8,128)(2,1)S(1)} %pad_maximum_fusion.3), channel_id=1, source_target_pairs={{0,8},{8,16},{16,24},{1,9},{9,17},{17,25},{2,10},{10,18},{18,26},{... | collective-permute-start | bytes 98312 | tf_op jit(solution)/shard_map/ppermute | solution.py:18
  21.9 1.6 copy-start.2
  28.5 251.6 %reduce-scatter.5.cloned.1.call-start = ((), (), s32[]{:S(2)}) async-start(), calls=%async_computation.4 | async-start | bytes 4325376 | tf_op jit(solution)/shard_map/reduce_scatter | solution.py:153
  117.3 8.6 %slice-start = ((s8[8912896]{0:T(1024)(128)(4,1)}), s8[4194304]{0:T(1024)(128)(4,1)S(1)}, s32[]{:S(2)}) async-start(s8[8912896]{0:T(1024)(128)(4,1)} %bitcast.54), calls=%async_computation.5 | async-start | bytes 8388608
  117.7 8.2 %slice-start.1 = ((s8[8912896]{0:T(1024)(128)(4,1)}), s8[4194304]{0:T(1024)(128)(4,1)S(1)}, s32[]{:S(2)}) async-start(s8[8912896]{0:T(1024)(128)(4,1)} %bitcast.54), calls=%async_computation.6 | async-start | bytes 8388608
  117.7 8.2 %slice-start.2 = ((s8[8912896]{0:T(1024)(128)(4,1)}), s8[524288]{0:T(1024)(128)(4,1)S(1)}, s32[]{:S(2)}) async-start(s8[8912896]{0:T(1024)(128)(4,1)} %bitcast.54), calls=%async_computation.7 | async-start | bytes 1048576
  117.7 8.2 %copy-start.3 = (bf16[1,2048,896]{2,1,0:T(8,128)(2,1)S(1)}, bf16[1,2048,896]{2,1,0:T(8,128)(2,1)}, u32[]{:S(2)}) copy-start(bf16[1,2048,896]{2,1,0:T(8,128)(2,1)} %param.21) | copy-start | bytes 11010052
  125.9 4.8 %copy-start.4 = (bf16[1,896,2048]{2,1,0:T(8,128)(2,1)S(1)}, bf16[1,896,2048]{2,1,0:T(8,128)(2,1)}, u32[]{:S(2)}) copy-start(bf16[1,896,2048]{2,1,0:T(8,128)(2,1)} %param.23) | copy-start | bytes 11010052
Sparse Core Ops, SparseCore 0:
  13.0 103.1 all-gather.1
Sparse Core Ops, SparseCore 1:
  28.6 76.8 reduce-scatter.2
  136.9 143.1 reduce-scatter.4
